TPU v7x, 32 devices: a whole 2x2x4 slice. The times are simulated.
32 devices in a mesh: ep: 16 (over z, y, x), tp: 2 (over core).
Axes of the slice: x: 2, y: 2, z: 4, core: 2. Of those that a mesh axis runs over, the one named last changes fastest.
Arguments:
- tokens: bfloat16 [384, 2048], P('ep'), may hold values from -40 to 40
- old_state: float32 [384, 16, 4096], P('ep', 'tp'), may hold values from -6 to 6
- w_query: bfloat16 [2048, 1024], P(None, 'tp'), may hold values from -0.125 to 0.125
- w_forget: bfloat16 [2048, 1024], P(None, 'tp'), may hold values from -0.125 to 0.125
- w_value: bfloat16 [2048, 1024], P(None, 'tp'), may hold values from -0.125 to 0.125
- w_gate: bfloat16 [2048, 1024], P(None, 'tp'), may hold values from -0.125 to 0.125
- lower_bound: float32 [1024], P('tp'), may hold values from 0.05 to 0.9
- head_gain: float32 [64], replicated, may hold values from 0.1 to 1.9
- w_out: bfloat16 [1024, 2048], P('tp'), may hold values from -0.1875 to 0.1875
- mix_gain: float32 [2048], replicated, may hold values from 0.1 to 1.9
- expert_gate: bfloat16 [16, 2048, 512], P('ep', None, 'tp'), may hold values from -0.125 to 0.125
- expert_up: bfloat16 [16, 2048, 512], P('ep', None, 'tp'), may hold values from -0.125 to 0.125
- expert_down: bfloat16 [16, 512, 2048], P('ep', 'tp'), may hold values from -0.25 to 0.25
- expert_ids: int32 [384, 2], P('ep'), may hold values from 0 to 15, as said below
- route_weight: float32 [384, 2], P('ep'), may hold values from 0.1 to 1
- moe_gain: float32 [2048], replicated, may hold values from 0.1 to 1.9
Outputs:
- next_tokens: bfloat16 [384, 2048], P('ep', 'tp')
- new_state: float32 [384, 16, 4096], P('ep', 'tp')
Inputs may be any that keep to these rules, and one draw needn't show every extreme that they name: `expert_ids`: each row names two different experts of one group of 4 consecutive experts. In each aligned block of 24 rows no expert is named by more than 6 rows, and one expert, the same in every block, is named by exactly 6 rows of every block.
All inputs are finite; a program needn't handle non-finite values.
Results may differ from a plain program's by a relative error of at most 0.011.
Values may be sent and summed in bfloat16 or wider, within the bound.
A program may use at most 128 MiB of HBM per device.

v0:
```python
import jax
import jax.numpy as jnp
from jax import lax
from jax.sharding import PartitionSpec as P


def layer_normed(values, gain):
    center = jnp.mean(values, -1, keepdims=True)
    centered = values - center
    variance = jnp.mean(centered * centered, -1, keepdims=True)
    return centered * lax.rsqrt(variance + 1e-05) * gain


def rounded(values):
    return lax.optimization_barrier(values.astype(jnp.bfloat16)).astype(jnp.float32)


def slot_table(ids_block, expert_count, capacity):
    flat_ids = ids_block.reshape(-1)
    onehot = (flat_ids[:, None] == jnp.arange(expert_count, dtype=jnp.int32)[None, :]).astype(
        jnp.int32
    )
    before = jnp.cumsum(onehot, 0) - onehot
    rank = jnp.sum(before * onehot, 1)
    return flat_ids * capacity + rank


def per_device(
    tokens,
    old_state,
    w_query,
    w_forget,
    w_value,
    w_gate,
    lower_bound,
    head_gain,
    w_out,
    mix_gain,
    expert_gate,
    expert_up,
    expert_down,
    expert_ids,
    route_weight,
    moe_gain,
):
    row_count, model_width = tokens.shape
    heads_here = old_state.shape[1]
    head_dim = head_gain.shape[0]
    head_cols = w_query.shape[1]
    q_lin = jnp.dot(tokens, w_query, preferred_element_type=jnp.float32)
    f_lin = jnp.dot(tokens, w_forget, preferred_element_type=jnp.float32)
    v_lin = jnp.dot(tokens, w_value, preferred_element_type=jnp.float32)
    g_lin = jnp.dot(tokens, w_gate, preferred_element_type=jnp.float32)
    act_query = jax.nn.silu(q_lin).reshape(row_count, heads_here, head_dim)
    bound = lower_bound.reshape(heads_here, head_dim)
    forget = bound + (1.0 - bound) * jax.nn.sigmoid(f_lin.reshape(row_count, heads_here, head_dim))
    previous = old_state.reshape(row_count, heads_here, head_dim, head_dim)
    new_state = forget[..., None] * previous + (1.0 - forget)[..., None] * v_lin.reshape(
        row_count, heads_here, 1, head_dim
    )
    readout = jnp.einsum("shi,shij->shj", act_query, new_state, precision=lax.Precision.HIGHEST)
    normed = readout * lax.rsqrt(jnp.mean(readout * readout, -1, keepdims=True) + 1e-06) * head_gain
    mixer_out = (
        (normed * jax.nn.silu(g_lin.reshape(row_count, heads_here, head_dim)))
        .reshape(row_count, head_cols)
        .astype(jnp.bfloat16)
    )
    own_part = rounded(jnp.dot(mixer_out, w_out, preferred_element_type=jnp.float32))
    mixed = lax.psum(own_part.astype(jnp.bfloat16), "tp").astype(jnp.float32)
    after_mixer = layer_normed(tokens.astype(jnp.float32) + mixed, mix_gain).astype(jnp.bfloat16)
    expert_count = lax.axis_size("ep")
    core_count = lax.axis_size("tp")
    top_count = expert_ids.shape[1]
    capacity = max(2, 2 * top_count * row_count // expert_count)
    slot_ids = slot_table(expert_ids, expert_count, capacity)
    choose = (
        slot_ids[None, :] == jnp.arange(expert_count * capacity, dtype=jnp.int32)[:, None]
    ).astype(jnp.bfloat16)
    choose = choose.reshape(expert_count * capacity, row_count, top_count).sum(-1)
    outgoing = jnp.dot(choose, after_mixer, preferred_element_type=jnp.float32).astype(jnp.bfloat16)
    outgoing = outgoing.reshape(expert_count, capacity, model_width)
    arrived = lax.all_to_all(outgoing, "ep", split_axis=0, concat_axis=0, tiled=True)
    sources = arrived.shape[0]
    slots_now = arrived.shape[1]
    rows_in = arrived.reshape(sources * slots_now, model_width)
    gate_act = jnp.dot(rows_in, expert_gate[0], preferred_element_type=jnp.float32)
    up_act = jnp.dot(rows_in, expert_up[0], preferred_element_type=jnp.float32)
    hidden = (jax.nn.silu(gate_act) * up_act).astype(jnp.bfloat16)
    partial_rows = rounded(jnp.dot(hidden, expert_down[0], preferred_element_type=jnp.float32))
    summed_rows = lax.psum_scatter(
        partial_rows.astype(jnp.bfloat16), "tp", scatter_dimension=1, tiled=True
    ).astype(jnp.float32)
    results = summed_rows.astype(jnp.bfloat16).reshape(sources, slots_now, summed_rows.shape[1])
    back_half = lax.all_to_all(results, "ep", split_axis=0, concat_axis=0, tiled=True)
    returned = lax.all_gather(back_half, "tp", axis=2, tiled=True)
    flat_back = returned.reshape(expert_count * capacity, model_width)
    picked = (
        jnp.take(flat_back, slot_ids, axis=0)
        .reshape(row_count, top_count, model_width)
        .astype(jnp.float32)
    )
    moe_sum = jnp.sum(picked * route_weight[..., None], 1)
    full_rows = layer_normed(after_mixer.astype(jnp.float32) + moe_sum, moe_gain).astype(
        jnp.bfloat16
    )
    half_width = model_width // core_count
    next_tokens = lax.dynamic_slice_in_dim(
        full_rows, lax.axis_index("tp") * half_width, half_width, 1
    )
    return (next_tokens, new_state.reshape(row_count, heads_here, head_dim * head_dim))


def solution(mesh):
    in_specs = (
        P("ep", None),
        P("ep", "tp", None),
        P(None, "tp"),
        P(None, "tp"),
        P(None, "tp"),
        P(None, "tp"),
        P("tp"),
        P(),
        P("tp", None),
        P(),
        P("ep", None, "tp"),
        P("ep", None, "tp"),
        P("ep", "tp", None),
        P("ep", None),
        P("ep", None),
        P(),
    )
    out_specs = (P("ep", "tp"), P("ep", "tp", None))
    return jax.shard_map(
        per_device, mesh=mesh, in_specs=in_specs, out_specs=out_specs, check_vma=False
    )
```

profile of v0, /device:TPU:0, one launch (start us, length us, event | category | flops | bytes accessed | tf_op | source)
XLA Modules:
  0.0 128.8 jit_solution(17914694816942390285)
XLA Ops:
  7.2 0.9 add.128
  8.1 2.1 %fusion.7 = f32[24,512]{1,0:T(8,128)S(1)} fusion(bf16[24,2048]{1,0:T(8,128)(2,1)} %param.16, bf16[2048,512]{1,0:T(8,128)(2,1)} %param.19), kind=kOutput, calls=%fused_computation.15 | convolution fusion | flops 50368512 | bytes 2244608 | tf_op jit(solution)/shard_map/dot_general | solution.py:51
  10.3 2.0 %fusion.33 = f32[24,512]{1,0:T(8,128)S(1)} fusion(bf16[24,2048]{1,0:T(8,128)(2,1)} %param.16, bf16[2048,512]{1,0:T(8,128)(2,1)} %param.20), kind=kOutput, calls=%fused_computation.66 | convolution fusion | flops 50331648 | bytes 2244608 | tf_op jit(solution)/shard_map/dot_general | solution.py:52
  12.3 0.1 mul.165
  12.4 6.1 %reshape.162 = f32[24,8,64,64]{3,2,1,0:T(8,128)} reshape(f32[24,8,4096]{2,1,0:T(8,128)} %param.17) | data formatting | bytes 6291456 | tf_op jit(solution)/shard_map/reshape | solution.py:57
  18.5 2.0 %divide_multiply_fusion = f32[24,512]{1,0:T(8,128)S(1)} fusion(bf16[24,2048]{1,0:T(8,128)(2,1)S(1)} %copy-done.1, bf16[2048,512]{1,0:T(8,128)(2,1)} %param.18), kind=kOutput, calls=%fused_computation.44 | convolution fusion | flops 50380800 | bytes 2244608 | tf_op jit(solution)/shard_map/dot_general | solution.py:50
  20.7 9.6 %fusion = f32[24,8,1,64]{3,2,1,0:T(1,128)S(1)} fusion(f32[24,8,64,1]{2,3,1,0:T(1,128)S(1)} %bitcast.40, f32[24,8,64,64]{3,2,1,0:T(8,128)} %reshape.162, f32[24,8,64]{2,1,0:T(8,128)S(1)} %get-tuple-element.7, f32[24,8,64]{2,1,0:T(8,128)S(1)} %mul.165, f32[24,8,64]{2,1,0:T(8,128)S(1)} %get-tuple-element.6), kind=kOutput, calls=%fused_computation.1 | convolution fusion | flops 11796480 | bytes 3391488 | tf_op jit(solution)/shard_map/shi,shij->shj/dot_general | solution.py:61
  30.3 0.1 multiply_reduce_fusion.3
  30.4 0.4 fusion.34
  30.8 0.1 reshape.163
  30.9 0.1 multiply_convert_fusion.1
  31.0 0.1 convert_element_type.53
  31.1 1.0 convolution_convert_fusion.2
  32.2 0.1 copy.28
  32.3 0.1 reshape.164
  32.6 0.2 select_reduce_fusion
  32.7 0.1 reduce_sum.83
  33.0 19.9 %all-reduce.2.cloned.1.call-done = bf16[24,2048]{1,0:T(8,128)(2,1)} async-done(((bf16[24,2048]{1,0:T(8,128)(2,1)}), bf16[24,2048]{1,0:T(8,128)(2,1)}) %all-reduce.2.cloned.1.call-update) | async-done | bytes 98320 | tf_op jit(solution)/shard_map/psum | solution.py:69
  52.9 1.0 fusion.14
  53.9 1.1 multiply_reduce_fusion.2
  55.1 1.0 multiply_convert_fusion
  56.1 0.3 convolution_convert_fusion.1
  56.4 0.9 reshape.165
  57.3 6.8 %all-to-all-start = ((bf16[16,6,2048]{2,1,0:T(8,128)(2,1)}), bf16[16,6,2048]{2,1,0:T(8,128)(2,1)S(1)}, u32[]{:S(2)}, u32[]{:S(2)}) async-start(bf16[16,6,2048]{2,1,0:T(8,128)(2,1)} %reshape.165), calls=%async_computation | async-start | bytes 1048576 | tf_op jit(solution)/shard_map/all_to_all | solution.py:82
  64.2 3.8 %broadcast_multiply_fusion = f32[24,8,64,64]{3,2,1,0:T(8,128)} fusion(f32[24,8,64]{2,1,0:T(8,128)S(1)} %mul.165, f32[24,8,64]{2,1,0:T(8,128)S(1)} %get-tuple-element.6), kind=kLoop, calls=%fused_computation.5 | loop fusion | flops 786432 | bytes 3244032 | tf_op jit(solution)/shard_map/mul | solution.py:58
  68.0 5.8 %mul.196 = f32[24,8,4096]{2,1,0:T(8,128)} reshape(f32[24,8,64,64]{3,2,1,0:T(8,128)} %broadcast_multiply_fusion) | data formatting | bytes 6291456 | tf_op jit(solution)/shard_map/mul | solution.py:58
  73.8 3.8 %mul.162 = f32[24,8,64,64]{3,2,1,0:T(8,128)} broadcast(f32[24,8,64]{2,1,0:T(8,128)S(1)} %get-tuple-element.7), dimensions={0,1,2} | broadcast | bytes 3194880 | tf_op jit(solution)/shard_map/mul | solution.py:58
  77.6 5.9 %mul.194 = f32[24,8,4096]{2,1,0:T(8,128)} reshape(f32[24,8,64,64]{3,2,1,0:T(8,128)} %mul.162) | data formatting | bytes 6291456 | tf_op jit(solution)/shard_map/mul | solution.py:58
  83.5 0.1 reshape.166
  83.7 1.5 %fusion.11 = f32[96,256]{1,0:T(8,128)S(1)} fusion(bf16[96,2048]{1,0:T(8,128)(2,1)S(1)} %reshape.166, bf16[1,2048,256]{2,1,0:T(8,128)(2,1)} %param.26), kind=kOutput, calls=%fused_computation.18 | convolution fusion | flops 100663296 | bytes 1540096 | tf_op jit(solution)/shard_map/dot_general | solution.py:86
  85.2 3.1 %convolution_convert_fusion = bf16[96,2048]{1,0:T(8,128)(2,1)} fusion(bf16[96,2048]{1,0:T(8,128)(2,1)S(1)} %reshape.166, bf16[1,256,2048]{2,1,0:T(8,128)(2,1)} %param.28, bf16[1,2048,256]{2,1,0:T(8,128)(2,1)} %param.27, f32[96,256]{1,0:T(8,128)S(1)} %fusion.11), kind=kOutput, calls=%fused_computation.7 | convolution fusion | flops 201670656 | bytes 2981888 | tf_op jit(solution)/shard_map/dot_general | solution.py:89
  88.3 6.2 %multiply_add_fusion = f32[24,8,4096]{2,1,0:T(8,128)} fusion(f32[24,8,4096]{2,1,0:T(8,128)} %mul.196, f32[24,8,4096]{2,1,0:T(8,128)} %mul.194, f32[24,8,4096]{2,1,0:T(8,128)} %param.17), kind=kLoop, calls=%fused_computation.4 | loop fusion | flops 1572864 | bytes 12582912 | tf_op jit(solution)/shard_map/add | solution.py:58
  94.5 3.1 %reduce-scatter.2.cloned.1.call-done = bf16[96,1024]{1,0:T(8,128)(2,1)} async-done(((bf16[96,2048]{1,0:T(8,128)(2,1)}), bf16[96,1024]{1,0:T(8,128)(2,1)}) %reduce-scatter.2.cloned.1.call-update) | async-done | bytes 196624 | tf_op jit(solution)/shard_map/reduce_scatter | solution.py:90
  97.5 1.7 %reshape.167 = bf16[16,6,1024]{2,1,0:T(8,128)(2,1)} reshape(bf16[96,1024]{1,0:T(8,128)(2,1)} %reduce-scatter.2.cloned.1.call-done) | data formatting | bytes 393216 | tf_op jit(solution)/shard_map/reshape | solution.py:93
  99.2 6.7 %all-to-all-start.1 = ((bf16[16,6,1024]{2,1,0:T(8,128)(2,1)}), bf16[16,6,1024]{2,1,0:T(8,128)(2,1)S(1)}, u32[]{:S(2)}, u32[]{:S(2)}) async-start(bf16[16,6,1024]{2,1,0:T(8,128)(2,1)} %reshape.167), calls=%async_computation.2 | async-start | bytes 524288 | tf_op jit(solution)/shard_map/all_to_all | solution.py:94
  106.0 0.1 copy.31
  106.1 0.1 mul.185
  106.2 0.1 copy.30
  106.3 0.1 copy.32
  106.4 10.0 %all-to-all-done.1 = bf16[16,6,1024]{2,1,0:T(8,128)(2,1)S(1)} async-done(((bf16[16,6,1024]{2,1,0:T(8,128)(2,1)}), bf16[16,6,1024]{2,1,0:T(8,128)(2,1)S(1)}, u32[]{:S(2)}, u32[]{:S(2)}) %all-to-all-start.1) | async-done | bytes 196640 | tf_op jit(solution)/shard_map/all_to_all | solution.py:94
  116.4 2.2 %all_gather.3 = bf16[16,6,2048]{2,1,0:T(8,128)(2,1)S(1)} all-gather(bf16[16,6,1024]{2,1,0:T(8,128)(2,1)S(1)} %all-to-all-done.1), channel_id=1, replica_groups=mesh['ep'=16,'tp'=2] {'tp'}, dimensions={2}, use_global_device_ids=true | all-gather | bytes 589824 | tf_op jit(solution)/shard_map/all_gather | solution.py:95
  118.5 0.1 reshape.168
  118.7 0.7 gather_fusion
  119.4 0.1 gather.7
  119.5 1.4 %multiply_reduce_fusion = f32[24,2048]{1,0:T(8,128)S(1)} fusion(bf16[24,2,2048]{2,1,0:T(2,128)(2,1)S(1)} %gather.7, pred[24,2]{1,0:T(8,128)(4,1)S(1)} %copy.30, f32[24,2]{1,0:T(8,128)S(1)} %copy.32), kind=kLoop, calls=%fused_computation.20 | loop fusion | flops 344064 | bytes 393456 | tf_op jit(solution)/shard_map/reduce_sum | solution.py:102
  120.9 0.1 fusion.16
  121.0 0.2 multiply_reduce_fusion.1
  121.3 0.7 fusion.18
  (38 shorter events, 0.7 us)
Async XLA Ops:
  7.2 24.0 %copy-start = (bf16[512,2048]{1,0:T(8,128)(2,1)S(1)}, bf16[512,2048]{1,0:T(8,128)(2,1)}, u32[]{:S(2)}) copy-start(bf16[512,2048]{1,0:T(8,128)(2,1)} %param.24) | copy-start | bytes 6291460
  7.2 45.7 %all-reduce.2.cloned.1.call-start = ((), (), s32[]{:S(2)}) async-start(), calls=%async_computation.3 | async-start | bytes 196608 | tf_op jit(solution)/shard_map/psum | solution.py:69
  12.4 6.1 %copy-start.1 = (bf16[24,2048]{1,0:T(8,128)(2,1)S(1)}, bf16[24,2048]{1,0:T(8,128)(2,1)}, u32[]{:S(2)}) copy-start(bf16[24,2048]{1,0:T(8,128)(2,1)} %param.16) | copy-start | bytes 294916
  20.6 9.8 %copy-start.2 = (bf16[2048,512]{1,0:T(8,128)(2,1)S(1)}, bf16[2048,512]{1,0:T(8,128)(2,1)}, u32[]{:S(2)}) copy-start(bf16[2048,512]{1,0:T(8,128)(2,1)} %param.21) | copy-start | bytes 6291460
  20.7 10.3 %copy-start.6 = (f32[64]{0:T(128)S(1)}, f32[64]{0:T(128)}, u32[]{:S(2)}) copy-start(f32[64]{0:T(128)} %param.23) | copy-start | bytes 772
  30.3 1.9 %copy-start.3 = (s32[24,2]{0,1:T(2,128)S(1)}, s32[24,2]{0,1:T(2,128)}, u32[]{:S(2)}) copy-start(s32[24,2]{0,1:T(2,128)} %param.29) | copy-start | bytes 580
  30.3 24.8 %copy-start.4 = (f32[2048]{0:T(1024)S(1)}, f32[2048]{0:T(1024)}, u32[]{:S(2)}) copy-start(f32[2048]{0:T(1024)} %param.25) | copy-start | bytes 24580
  57.3 26.2 %all-to-all-start = ((bf16[16,6,2048]{2,1,0:T(8,128)(2,1)}), bf16[16,6,2048]{2,1,0:T(8,128)(2,1)S(1)}, u32[]{:S(2)}, u32[]{:S(2)}) async-start(bf16[16,6,2048]{2,1,0:T(8,128)(2,1)} %reshape.165), calls=%async_computation | async-start | bytes 1048576 | tf_op jit(solution)/shard_map/all_to_all | solution.py:82
  64.1 33.4 %reduce-scatter.2.cloned.1.call-start = ((), (), s32[]{:S(2)}) async-start(), calls=%async_computation.4 | async-start | bytes 589824 | tf_op jit(solution)/shard_map/reduce_scatter | solution.py:90
  88.3 18.0 %copy-start.5 = (f32[24,2]{0,1:T(2,128)S(1)}, f32[24,2]{0,1:T(2,128)}, u32[]{:S(2)}) copy-start(f32[24,2]{0,1:T(2,128)} %param.30) | copy-start | bytes 580
  99.2 17.1 %all-to-all-start.1 = ((bf16[16,6,1024]{2,1,0:T(8,128)(2,1)}), bf16[16,6,1024]{2,1,0:T(8,128)(2,1)S(1)}, u32[]{:S(2)}, u32[]{:S(2)}) async-start(bf16[16,6,1024]{2,1,0:T(8,128)(2,1)} %reshape.167), calls=%async_computation.2 | async-start | bytes 524288 | tf_op jit(solution)/shard_map/all_to_all | solution.py:94
  106.3 14.9 %dynamic-slice-start = ((f32[2048]{0:T(1024)}, s32[]{:T(128)}), f32[1024]{0:T(1024)S(1)}, s32[]{:S(2)}) async-start(f32[2048]{0:T(1024)} %param.31, s32[]{:T(128)} %select_n.28), calls=%async_computation.5 | async-start | bytes 8704 | tf_op jit(solution)/shard_map/dynamic_slice | solution.py:107
Sparse Core Ops, SparseCore 0:
  32.3 20.5 all-reduce.1
  88.4 9.0 reduce-scatter.1
where the time goes:
time: 130 us; the launch traced here: 129 us
  waiting for transfers between devices  33 us (25%)
  local copies, waits for them, and re-layouts  27.5 us (21%)
  matrix products  22 us (17%)
  other arithmetic  16.2 us (12%)
  between operations  14.3 us (11%)
  starting transfers between devices  13.6 us (10%)
  blocking collectives  2.17 us (2%)
    psum x1, waiting for transfers between devices, per_device(): mixed = lax.psum(own_part.astype(jnp.bfloat16), 'tp').astype(jnp.float32)  19.9 us
    all_to_all x1, waiting for transfers between devices, per_device(): lax.all_to_all(results, 'ep', split_axis=0, concat_axis=0, tiled=True)  9.99 us
    mul x2, local copies, waits for them, and re-layouts, per_device(): forget[..., None] * previous  9.72 us
    dot_general x1, matrix products, per_device(): jnp.einsum('shi,shij->shj', act_query, new_state, precision=lax.Precision...  9.61 us
    all_to_all x1, starting transfers between devices, per_device(): lax.all_to_all(outgoing, 'ep', split_axis=0, concat_axis=0, tiled=True)  6.82 us
    all_to_all x1, starting transfers between devices, per_device(): lax.all_to_all(results, 'ep', split_axis=0, concat_axis=0, tiled=True)  6.74 us
    add x1, other arithmetic, per_device(): forget[..., None] * previous  6.17 us
    reshape x1, local copies, waits for them, and re-layouts, per_device(): previous = old_state.reshape(row_count, heads_here, head_dim, head_dim)  6.14 us
  transfers between devices with their start and end apart: 4, of which 3 were waited for; matrix products, arithmetic and copies ran while one was open for 21% of the time, Pallas kernels for 0%

commit v1 on v0

--- a/solution.py
+++ b/solution.py
@@ -2,6 +2,11 @@
 import jax.numpy as jnp
 from jax import lax
 from jax.sharding import PartitionSpec as P
+
+
+def add_all(block, axis):
+    parts = lax.all_gather(block, axis)
+    return jnp.sum(parts, axis=0)
 
 
 def layer_normed(values, gain):
@@ -66,7 +71,7 @@
         .astype(jnp.bfloat16)
     )
     own_part = rounded(jnp.dot(mixer_out, w_out, preferred_element_type=jnp.float32))
-    mixed = lax.psum(own_part.astype(jnp.bfloat16), "tp").astype(jnp.float32)
+    mixed = add_all(own_part.astype(jnp.bfloat16), "tp").astype(jnp.float32)
     after_mixer = layer_normed(tokens.astype(jnp.float32) + mixed, mix_gain).astype(jnp.bfloat16)
     expert_count = lax.axis_size("ep")
     core_count = lax.axis_size("tp")

time: 130 us -> 110 us (0.85)
  waiting for transfers between devices: 33 us -> 13.1 us
  other arithmetic: 16.2 us -> 13.6 us
  blocking collectives: 2.17 us -> 4.25 us
  starting transfers between devices: 13.6 us -> 15 us
    psum x1 -> x0, waiting for transfers between devices: 19.9 us -> none  [per_device(): mixed = lax.psum(own_part.astype(jnp.bfloat16), 'tp').astype(jnp.float32)]
    all_gather x0 -> x1, blocking collectives: none -> 2.08 us  [add_all(): parts = lax.all_gather(block, axis)]
    all_to_all x1, starting transfers between devices: 6.82 us -> 8.21 us  [per_device(): lax.all_to_all(outgoing, 'ep', split_axis=0, concat_axis=0, tiled=True)]
  transfers between devices with their start and end apart: 4 -> 3, of which waited for: 3 -> 2; matrix products, arithmetic and copies ran while one was open for 21% -> 24% of each run, Pallas kernels for 0% -> 0%
where the time goes in v1:
time: 110 us; the launch traced here: 109 us
  local copies, waits for them, and re-layouts  27.5 us (25%)
  matrix products  21.3 us (19%)
  starting transfers between devices  15 us (14%)
  between operations  14.3 us (13%)
  other arithmetic  13.6 us (12%)
  waiting for transfers between devices  13.1 us (12%)
  blocking collectives  4.25 us (4%)
    all_to_all x1, waiting for transfers between devices, per_device(): lax.all_to_all(results, 'ep', split_axis=0, concat_axis=0, tiled=True)  9.97 us
    mul x2, local copies, waits for them, and re-layouts, per_device(): forget[..., None] * previous  9.72 us
    dot_general x1, matrix products, per_device(): jnp.einsum('shi,shij->shj', act_query, new_state, precision=lax.Precision...  9.61 us
    all_to_all x1, starting transfers between devices, per_device(): lax.all_to_all(outgoing, 'ep', split_axis=0, concat_axis=0, tiled=True)  8.21 us
    all_to_all x1, starting transfers between devices, per_device(): lax.all_to_all(results, 'ep', split_axis=0, concat_axis=0, tiled=True)  6.74 us
    add x1, other arithmetic, per_device(): forget[..., None] * previous  6.17 us
    reshape x1, local copies, waits for them, and re-layouts, per_device(): previous = old_state.reshape(row_count, heads_here, head_dim, head_dim)  6.14 us
    mul x2, local copies, waits for them, and re-layouts, per_device(): (1.0 - forget)[..., None]  5.92 us
  transfers between devices with their start and end apart: 3, of which 2 were waited for; matrix products, arithmetic and copies ran while one was open for 24% of the time, Pallas kernels for 0%

profile of v1, /device:TPU:0, one launch (start us, length us, event | category | flops | bytes accessed | tf_op | source)
XLA Modules:
  0.0 109.0 jit_solution(15690993807426451860)
XLA Ops:
  7.2 0.9 add.126
  8.1 2.1 %fusion.7 = f32[24,512]{1,0:T(8,128)S(1)} fusion(bf16[24,2048]{1,0:T(8,128)(2,1)} %param.16, bf16[2048,512]{1,0:T(8,128)(2,1)} %param.19), kind=kOutput, calls=%fused_computation.15 | convolution fusion | flops 50368512 | bytes 2244608 | tf_op jit(solution)/shard_map/dot_general | solution.py:56
  10.2 2.0 %fusion.33 = f32[24,512]{1,0:T(8,128)S(1)} fusion(bf16[24,2048]{1,0:T(8,128)(2,1)} %param.16, bf16[2048,512]{1,0:T(8,128)(2,1)} %param.20), kind=kOutput, calls=%fused_computation.66 | convolution fusion | flops 50331648 | bytes 2244608 | tf_op jit(solution)/shard_map/dot_general | solution.py:57
  12.3 0.1 mul.165
  12.4 6.1 %reshape.162 = f32[24,8,64,64]{3,2,1,0:T(8,128)} reshape(f32[24,8,4096]{2,1,0:T(8,128)} %param.17) | data formatting | bytes 6291456 | tf_op jit(solution)/shard_map/reshape | solution.py:62
  18.5 2.0 %divide_multiply_fusion = f32[24,512]{1,0:T(8,128)S(1)} fusion(bf16[24,2048]{1,0:T(8,128)(2,1)S(1)} %copy-done.1, bf16[2048,512]{1,0:T(8,128)(2,1)} %param.18), kind=kOutput, calls=%fused_computation.44 | convolution fusion | flops 50380800 | bytes 2244608 | tf_op jit(solution)/shard_map/dot_general | solution.py:55
  20.6 9.6 %fusion = f32[24,8,1,64]{3,2,1,0:T(1,128)S(1)} fusion(f32[24,8,64,1]{2,3,1,0:T(1,128)S(1)} %bitcast.42, f32[24,8,64,64]{3,2,1,0:T(8,128)} %reshape.162, f32[24,8,64]{2,1,0:T(8,128)S(1)} %get-tuple-element.7, f32[24,8,64]{2,1,0:T(8,128)S(1)} %mul.165, f32[24,8,64]{2,1,0:T(8,128)S(1)} %get-tuple-element.6), kind=kOutput, calls=%fused_computation.1 | convolution fusion | flops 11796480 | bytes 3391488 | tf_op jit(solution)/shard_map/shi,shij->shj/dot_general | solution.py:66
  30.3 0.1 multiply_reduce_fusion.3
  30.4 0.4 fusion.34
  30.8 0.1 reshape.163
  30.9 0.1 multiply_convert_fusion.1
  31.0 0.1 convert_element_type.55
  31.1 0.4 convolution_convert_fusion.2
  31.5 2.1 %all-gather = bf16[48,2048]{1,0:T(8,128)(2,1)S(1)} all-gather(bf16[24,2048]{1,0:T(8,128)(2,1)S(1)} %convolution_convert_fusion.2), channel_id=2, replica_groups=mesh['ep'=16,'tp'=2] {'tp'}, dimensions={0}, use_global_device_ids=true | all-gather | bytes 294912 | tf_op jit(solution)/shard_map/all_gather | solution.py:8
  33.6 0.1 fusion.14
  33.8 0.2 multiply_reduce_fusion.2
  34.0 0.1 copy.28
  34.1 0.1 reshape.164
  34.3 0.2 select_reduce_fusion
  34.5 0.1 reduce_sum.96
  34.8 0.1 multiply_convert_fusion
  34.9 0.3 convolution_convert_fusion.1
  35.2 0.9 reshape.165
  36.1 8.2 %all-to-all-start = ((bf16[16,6,2048]{2,1,0:T(8,128)(2,1)}), bf16[16,6,2048]{2,1,0:T(8,128)(2,1)S(1)}, u32[]{:S(2)}, u32[]{:S(2)}) async-start(bf16[16,6,2048]{2,1,0:T(8,128)(2,1)} %reshape.165), calls=%async_computation | async-start | bytes 1048576 | tf_op jit(solution)/shard_map/all_to_all | solution.py:87
  44.4 3.8 %broadcast_multiply_fusion = f32[24,8,64,64]{3,2,1,0:T(8,128)} fusion(f32[24,8,64]{2,1,0:T(8,128)S(1)} %mul.165, f32[24,8,64]{2,1,0:T(8,128)S(1)} %get-tuple-element.6), kind=kLoop, calls=%fused_computation.5 | loop fusion | flops 786432 | bytes 3244032 | tf_op jit(solution)/shard_map/mul | solution.py:63
  48.2 5.8 %mul.196 = f32[24,8,4096]{2,1,0:T(8,128)} reshape(f32[24,8,64,64]{3,2,1,0:T(8,128)} %broadcast_multiply_fusion) | data formatting | bytes 6291456 | tf_op jit(solution)/shard_map/mul | solution.py:63
  54.0 3.8 %mul.162 = f32[24,8,64,64]{3,2,1,0:T(8,128)} broadcast(f32[24,8,64]{2,1,0:T(8,128)S(1)} %get-tuple-element.7), dimensions={0,1,2} | broadcast | bytes 3194880 | tf_op jit(solution)/shard_map/mul | solution.py:63
  57.8 5.9 %mul.194 = f32[24,8,4096]{2,1,0:T(8,128)} reshape(f32[24,8,64,64]{3,2,1,0:T(8,128)} %mul.162) | data formatting | bytes 6291456 | tf_op jit(solution)/shard_map/mul | solution.py:63
  63.7 0.1 reshape.166
  63.9 1.5 %fusion.11 = f32[96,256]{1,0:T(8,128)S(1)} fusion(bf16[96,2048]{1,0:T(8,128)(2,1)S(1)} %reshape.166, bf16[1,2048,256]{2,1,0:T(8,128)(2,1)} %param.26), kind=kOutput, calls=%fused_computation.18 | convolution fusion | flops 100663296 | bytes 1540096 | tf_op jit(solution)/shard_map/dot_general | solution.py:91
  65.4 3.1 %convolution_convert_fusion = bf16[96,2048]{1,0:T(8,128)(2,1)} fusion(bf16[96,2048]{1,0:T(8,128)(2,1)S(1)} %reshape.166, bf16[1,256,2048]{2,1,0:T(8,128)(2,1)} %param.28, bf16[1,2048,256]{2,1,0:T(8,128)(2,1)} %param.27, f32[96,256]{1,0:T(8,128)S(1)} %fusion.11), kind=kOutput, calls=%fused_computation.7 | convolution fusion | flops 201670656 | bytes 2981888 | tf_op jit(solution)/shard_map/dot_general | solution.py:94
  68.5 6.2 %multiply_add_fusion = f32[24,8,4096]{2,1,0:T(8,128)} fusion(f32[24,8,4096]{2,1,0:T(8,128)} %mul.196, f32[24,8,4096]{2,1,0:T(8,128)} %mul.194, f32[24,8,4096]{2,1,0:T(8,128)} %param.17), kind=kLoop, calls=%fused_computation.4 | loop fusion | flops 1572864 | bytes 12582912 | tf_op jit(solution)/shard_map/add | solution.py:63
  74.7 3.1 %reduce-scatter.2.cloned.1.call-done = bf16[96,1024]{1,0:T(8,128)(2,1)} async-done(((bf16[96,2048]{1,0:T(8,128)(2,1)}), bf16[96,1024]{1,0:T(8,128)(2,1)}) %reduce-scatter.2.cloned.1.call-update) | async-done | bytes 196624 | tf_op jit(solution)/shard_map/reduce_scatter | solution.py:95
  77.7 1.7 %reshape.167 = bf16[16,6,1024]{2,1,0:T(8,128)(2,1)} reshape(bf16[96,1024]{1,0:T(8,128)(2,1)} %reduce-scatter.2.cloned.1.call-done) | data formatting | bytes 393216 | tf_op jit(solution)/shard_map/reshape | solution.py:98
  79.4 6.7 %all-to-all-start.1 = ((bf16[16,6,1024]{2,1,0:T(8,128)(2,1)}), bf16[16,6,1024]{2,1,0:T(8,128)(2,1)S(1)}, u32[]{:S(2)}, u32[]{:S(2)}) async-start(bf16[16,6,1024]{2,1,0:T(8,128)(2,1)} %reshape.167), calls=%async_computation.2 | async-start | bytes 524288 | tf_op jit(solution)/shard_map/all_to_all | solution.py:99
  86.2 0.1 copy.31
  86.3 0.1 mul.185
  86.4 0.1 copy.30
  86.5 0.1 copy.32
  86.6 10.0 %all-to-all-done.1 = bf16[16,6,1024]{2,1,0:T(8,128)(2,1)S(1)} async-done(((bf16[16,6,1024]{2,1,0:T(8,128)(2,1)}), bf16[16,6,1024]{2,1,0:T(8,128)(2,1)S(1)}, u32[]{:S(2)}, u32[]{:S(2)}) %all-to-all-start.1) | async-done | bytes 196640 | tf_op jit(solution)/shard_map/all_to_all | solution.py:99
  96.6 2.2 %all_gather.11 = bf16[16,6,2048]{2,1,0:T(8,128)(2,1)S(1)} all-gather(bf16[16,6,1024]{2,1,0:T(8,128)(2,1)S(1)} %all-to-all-done.1), channel_id=1, replica_groups=mesh['ep'=16,'tp'=2] {'tp'}, dimensions={2}, use_global_device_ids=true | all-gather | bytes 589824 | tf_op jit(solution)/shard_map/all_gather | solution.py:100
  98.7 0.1 reshape.168
  98.9 0.7 gather_fusion
  99.6 0.1 gather.7
  99.7 1.4 %multiply_reduce_fusion = f32[24,2048]{1,0:T(8,128)S(1)} fusion(bf16[24,2,2048]{2,1,0:T(2,128)(2,1)S(1)} %gather.7, pred[24,2]{1,0:T(8,128)(4,1)S(1)} %copy.30, f32[24,2]{1,0:T(8,128)S(1)} %copy.32), kind=kLoop, calls=%fused_computation.20 | loop fusion | flops 344064 | bytes 393456 | tf_op jit(solution)/shard_map/reduce_sum | solution.py:107
  101.1 0.1 fusion.16
  101.3 0.2 multiply_reduce_fusion.1
  101.5 0.7 fusion.18
  (37 shorter events, 0.7 us)
Async XLA Ops:
  7.2 23.9 %copy-start = (bf16[512,2048]{1,0:T(8,128)(2,1)S(1)}, bf16[512,2048]{1,0:T(8,128)(2,1)}, u32[]{:S(2)}) copy-start(bf16[512,2048]{1,0:T(8,128)(2,1)} %param.24) | copy-start | bytes 6291460
  12.4 6.1 %copy-start.1 = (bf16[24,2048]{1,0:T(8,128)(2,1)S(1)}, bf16[24,2048]{1,0:T(8,128)(2,1)}, u32[]{:S(2)}) copy-start(bf16[24,2048]{1,0:T(8,128)(2,1)} %param.16) | copy-start | bytes 294916
  20.6 9.8 %copy-start.2 = (bf16[2048,512]{1,0:T(8,128)(2,1)S(1)}, bf16[2048,512]{1,0:T(8,128)(2,1)}, u32[]{:S(2)}) copy-start(bf16[2048,512]{1,0:T(8,128)(2,1)} %param.21) | copy-start | bytes 6291460
  20.6 10.3 %copy-start.6 = (f32[64]{0:T(128)S(1)}, f32[64]{0:T(128)}, u32[]{:S(2)}) copy-start(f32[64]{0:T(128)} %param.23) | copy-start | bytes 772
  30.3 3.7 %copy-start.3 = (s32[24,2]{0,1:T(2,128)S(1)}, s32[24,2]{0,1:T(2,128)}, u32[]{:S(2)}) copy-start(s32[24,2]{0,1:T(2,128)} %param.29) | copy-start | bytes 580
  30.3 4.5 %copy-start.4 = (f32[2048]{0:T(1024)S(1)}, f32[2048]{0:T(1024)}, u32[]{:S(2)}) copy-start(f32[2048]{0:T(1024)} %param.25) | copy-start | bytes 24580
  36.1 27.6 %all-to-all-start = ((bf16[16,6,2048]{2,1,0:T(8,128)(2,1)}), bf16[16,6,2048]{2,1,0:T(8,128)(2,1)S(1)}, u32[]{:S(2)}, u32[]{:S(2)}) async-start(bf16[16,6,2048]{2,1,0:T(8,128)(2,1)} %reshape.165), calls=%async_computation | async-start | bytes 1048576 | tf_op jit(solution)/shard_map/all_to_all | solution.py:87
  44.3 33.4 %reduce-scatter.2.cloned.1.call-start = ((), (), s32[]{:S(2)}) async-start(), calls=%async_computation.3 | async-start | bytes 589824 | tf_op jit(solution)/shard_map/reduce_scatter | solution.py:95
  68.5 18.0 %copy-start.5 = (f32[24,2]{0,1:T(2,128)S(1)}, f32[24,2]{0,1:T(2,128)}, u32[]{:S(2)}) copy-start(f32[24,2]{0,1:T(2,128)} %param.30) | copy-start | bytes 580
  79.4 17.1 %all-to-all-start.1 = ((bf16[16,6,1024]{2,1,0:T(8,128)(2,1)}), bf16[16,6,1024]{2,1,0:T(8,128)(2,1)S(1)}, u32[]{:S(2)}, u32[]{:S(2)}) async-start(bf16[16,6,1024]{2,1,0:T(8,128)(2,1)} %reshape.167), calls=%async_computation.2 | async-start | bytes 524288 | tf_op jit(solution)/shard_map/all_to_all | solution.py:99
  86.6 14.9 %dynamic-slice-start = ((f32[2048]{0:T(1024)}, s32[]{:T(128)}), f32[1024]{0:T(1024)S(1)}, s32[]{:S(2)}) async-start(f32[2048]{0:T(1024)} %param.31, s32[]{:T(128)} %select_n.28), calls=%async_computation.4 | async-start | bytes 8704 | tf_op jit(solution)/shard_map/dynamic_slice | solution.py:112
Sparse Core Ops, SparseCore 0:
  68.6 9.0 reduce-scatter.1
